TPU v7x, 32 devices: a whole 2x2x4 slice. The times are simulated.
32 devices in a mesh: row: 8 (over z, core), col: 4 (over y, x).
Axes of the slice: x: 2, y: 2, z: 4, core: 2. Of those that a mesh axis runs over, the one named last changes fastest.
Arguments:
- tokens: bfloat16 [4096, 4096], P('row', 'col'), may hold values from -6 to 6
- norm_gain: float32 [4096], replicated, may hold values from 0.1 to 1.9
- out_weight: bfloat16 [4096, 4096], P(None, 'col'), may hold values from -0.09375 to 0.09375
Outputs:
- mixed: bfloat16 [4096, 4096], P('row', 'col')
All inputs are finite; a program needn't handle non-finite values.
Results may differ from a plain program's by a relative error of at most 0.015.
Values may be sent and summed in bfloat16 or wider, within the bound.
A program may use at most 64 MiB of HBM per device.

v0:
```python
import functools
import math

import numpy as np

import jax
import jax.numpy as jnp
from jax import lax
from jax.experimental import pallas as pl
from jax.experimental.pallas import tpu as pltpu
from jax.sharding import PartitionSpec as P

GROUPS = 4


EPSILON = 1e-06
PRECISE = lax.Precision.HIGHEST


def phases(left_idx, right_idx, period):
    product = left_idx[:, None] * right_idx[None, :] % period
    angles = product.astype(jnp.float32) * (2.0 * math.pi / period)
    return (jnp.cos(angles), jnp.sin(angles))


def split_table(table):
    table_high = table.astype(jnp.bfloat16)
    remainder = table - table_high.astype(jnp.float32)
    table_middle = remainder.astype(jnp.bfloat16)
    table_low = (remainder - table_middle.astype(jnp.float32)).astype(jnp.bfloat16)
    return (table_high, table_middle, table_low)


def host_tables(group_len, row_count, block_len):
    seq_len = block_len * row_count
    half = group_len // 2 // row_count
    slot = np.arange(group_len)
    freq = (slot // (2 * half)) * half + slot % half
    odd = slot // half % 2 == 1
    nyquist = odd & (freq == 0)
    sine = odd & ~nyquist
    freq = np.where(nyquist, group_len // 2, freq)
    chan = np.arange(group_len)
    angle = 2 * np.pi * (chan[:, None] * freq[None, :] % group_len) / group_len
    chan_table = np.where(sine[None, :], np.sin(angle), np.cos(angle)) / np.sqrt(group_len)
    low = np.arange(block_len)
    angle = 2 * np.pi * (low[:, None] * low[None, :] % block_len) / block_len
    low_table = np.concatenate([np.cos(angle), np.sin(angle)], 1) / np.sqrt(seq_len)
    high = np.arange(row_count)
    angle = 2 * np.pi * (high[:, None] * low[None, :] % seq_len) / seq_len
    return chan_table, low_table, np.cos(angle), np.sin(angle)


def slot_facts(slot, group_len, row_count):
    half = group_len // 2 // row_count
    freq = (slot // (2 * half)) * half + slot % half
    odd = slot // half % 2 == 1
    nyquist = odd & (freq == 0)
    return jnp.where(nyquist, group_len // 2, freq), odd & ~nyquist


def folding(group_len, row_count):
    freq, sine = slot_facts(jnp.arange(group_len, dtype=jnp.int32), group_len, row_count)
    chan = jnp.arange(group_len, dtype=jnp.int32)[None, :]
    direct = chan == freq[:, None]
    mirror = chan == ((group_len - freq) % group_len)[:, None]
    signed = jnp.where(sine[:, None], -1.0, 1.0)
    return jnp.where(direct, signed, jnp.where(mirror, 1.0, 0.0)).astype(jnp.bfloat16)


def on_device_folded(tokens, norm_gain, out_weight):
    row_count = lax.axis_size("row")
    col_count = lax.axis_size("col")
    block_len, group_len = tokens.shape
    full_width = group_len * col_count
    slab = group_len // row_count
    out_width = out_weight.shape[1]
    chan_table, low_table, twist_cos, twist_sin = host_tables(group_len, row_count, block_len)
    chan_table = jnp.asarray(chan_table, jnp.bfloat16)
    low_table = jnp.asarray(low_table, jnp.bfloat16)
    twist_cos = jnp.asarray(twist_cos, jnp.float32)[:, :, None]
    twist_sin = jnp.asarray(twist_sin, jnp.float32)[:, :, None]
    values = tokens.astype(jnp.float32)
    total = lax.psum(jnp.sum(values * values, axis=-1), "col")
    inv_rms = lax.rsqrt(total / full_width + EPSILON)[:, None]
    gain = lax.dynamic_slice_in_dim(norm_gain, lax.axis_index("col") * group_len, group_len)
    normed = (values * inv_rms * gain).astype(jnp.bfloat16)
    chans = jnp.dot(normed, chan_table, preferred_element_type=jnp.float32).astype(jnp.bfloat16)
    moved = lax.all_to_all(chans, "row", split_axis=1, concat_axis=0, tiled=True)
    blocks = moved.reshape(row_count, block_len, slab).astype(jnp.float32)
    _, sine = slot_facts(
        lax.axis_index("row") * slab + jnp.arange(slab, dtype=jnp.int32), group_len, row_count
    )
    tops, bottoms = [], []
    for q in range(row_count):
        real, imag = 0.0, 0.0
        for a in range(row_count):
            angle = 2 * math.pi * (a * q % row_count) / row_count
            real = real + blocks[a] * round(math.cos(angle), 12)
            imag = imag - blocks[a] * round(math.sin(angle), 12)
        turned_real = real * twist_cos[q] + imag * twist_sin[q]
        turned_imag = imag * twist_cos[q] - real * twist_sin[q]
        tops.append(jnp.where(sine, -turned_imag, turned_real).astype(jnp.bfloat16))
        bottoms.append(jnp.where(sine, turned_real, turned_imag).astype(jnp.bfloat16))
    stacked = jnp.concatenate([jnp.concatenate(tops, 1), jnp.concatenate(bottoms, 1)], 0)
    lows = jnp.dot(low_table, stacked, preferred_element_type=jnp.float32).astype(jnp.bfloat16)
    back = lax.all_to_all(
        lows.reshape(row_count, block_len // row_count, row_count * slab),
        "row", split_axis=0, concat_axis=0, tiled=True,
    )
    gathered = lax.all_gather(back, "col", axis=0, tiled=False)
    fold = folding(group_len, row_count)
    folded = jnp.einsum(
        "sm,gme->gse", fold, out_weight.reshape(col_count, group_len, out_width),
        preferred_element_type=jnp.float32,
    ).astype(jnp.bfloat16)
    mapped = jnp.einsum(
        "gspql,gsle->pqe",
        gathered.reshape(col_count, row_count, block_len // row_count, row_count, slab),
        folded.reshape(col_count, row_count, slab, out_width),
        preferred_element_type=jnp.float32,
    )
    return mapped.astype(jnp.bfloat16).reshape(block_len, out_width)


MESH = pl.DeviceIdType.MESH
F32 = jnp.float32
BF16 = jnp.bfloat16


def fused_kernel(
    dims, x_ref, gain_ref, table_hbm, low_hbm, twist_hbm, w_hbm, out_ref,
    table_ref, low_ref, twist_in, twist_ref, w_ref, fold_ref, folded, send1, recv1, sums, stacked, send2, lhs, acc,
    w_sem, s_send, s_recv, a_send, a_recv, b_send, b_recv, g_send, g_recv, l_sem,
):
    row_count, col_count = dims
    block_len, group_len = x_ref.shape
    full_width = group_len * col_count
    slab = group_len // row_count
    half = slab // 2
    pair = 2 * slab
    chips = row_count // 2
    part = block_len // row_count
    out_width = out_ref.shape[2]
    r = lax.axis_index("row")
    c = lax.axis_index("col")
    z = r // 2
    other = 2 * z + 1 - r % 2
    x_next = 2 * (c // 2) + 1 - c % 2
    y_next = 2 * (1 - c // 2) + c % 2
    diagonal = 2 * (1 - c // 2) + 1 - c % 2
    col_peers = (x_next, y_next, diagonal)
    table_copy = pltpu.make_async_copy(table_hbm, table_ref, l_sem.at[2])
    w_copy = pltpu.make_async_copy(w_hbm, w_ref, w_sem)
    low_copy = pltpu.make_async_copy(low_hbm, low_ref, l_sem.at[3])
    twist_copy = pltpu.make_async_copy(twist_hbm, twist_in, l_sem.at[4])
    for copy in (table_copy, w_copy, low_copy, twist_copy):
        copy.start()

    barrier = pltpu.get_barrier_semaphore()
    for step in range(1, row_count):
        pl.semaphore_signal(
            barrier, inc=1, device_id=(lax.rem(r + step, row_count), c), device_id_type=MESH
        )
    for peer in col_peers:
        pl.semaphore_signal(barrier, inc=1, device_id=(r, peer), device_id_type=MESH)
    values = x_ref[...].astype(F32)
    squares = values * values
    top = squares.astype(BF16)
    rest = (squares - top.astype(F32)).astype(BF16)
    ones = jnp.ones((16, group_len), BF16)
    lanes = (((1,), (1,)), ((), ()))
    own = lax.dot_general(ones, top, lanes, preferred_element_type=F32)
    own = own + lax.dot_general(ones, rest, lanes, preferred_element_type=F32)
    sums[c] = own[:8]
    pl.semaphore_wait(barrier, row_count + col_count - 2)
    sum_copies = []
    for k, peer in enumerate(col_peers):
        copy = pltpu.make_async_remote_copy(
            src_ref=sums.at[c], dst_ref=sums.at[c], send_sem=s_send.at[k], recv_sem=s_recv.at[k],
            device_id=(r, peer), device_id_type=MESH,
        )
        copy.start()
        sum_copies.append(copy)

    gain = gain_ref[:, pl.ds(pl.multiple_of(c * group_len, group_len), group_len)]
    scaled = (values * gain).astype(BF16)
    far_first = sorted(range(chips), key=lambda d: -min(d, chips - d))
    first_copies = []
    inv = None
    table_copy.wait()
    for d in far_first:
        chip = lax.rem(z + d, chips)
        product = jnp.dot(
            scaled, table_ref[:, pl.ds(pl.multiple_of(chip * pair, pair), pair)],
            preferred_element_type=F32,
        )
        if inv is None:
            for copy in sum_copies:
                copy.wait_recv()
            total = sums[0, :1, :]
            for k in range(1, col_count):
                total = total + sums[k, :1, :]
            inv = lax.rsqrt(total / full_width + EPSILON)
            inv = jnp.transpose(jnp.broadcast_to(inv, (128, block_len)))
        send1[2 * chip] = (product[:, :slab] * inv).astype(BF16)
        send1[2 * chip + 1] = (product[:, slab:] * inv).astype(BF16)
        for target, slot in ([(2 * chip, 2 * d), (2 * chip + 1, 2 * d + 1)] if d else [(other, 0)]):
            copy = pltpu.make_async_remote_copy(
                src_ref=send1.at[target], dst_ref=recv1.at[r], send_sem=a_send.at[slot],
                recv_sem=a_recv.at[slot] if d == 0 else a_recv.at[2 * d + r % 2],
                device_id=(target, c), device_id_type=MESH,
            )
            copy.start()
            first_copies.append(copy)
    stay1 = pltpu.make_async_copy(send1.at[r], recv1.at[r], l_sem.at[0])
    stay1.start()

    for t in range(chips):
        slot = t * pair + lax.broadcasted_iota(jnp.int32, (pair, 4 * slab), 0)
        column = lax.broadcasted_iota(jnp.int32, (pair, 4 * slab), 1)
        within = slot % slab
        freq = (slot // slab) * half + within % half
        odd = within >= half
        nyquist = odd & (freq == 0)
        high = min(group_len - slab * (t + 1), group_len - pair)
        direct = (column == freq - slab * t) & ~nyquist & (column < slab)
        mirror = (column - slab + high == group_len - freq) & (freq > 0)
        mirror = mirror & (column >= slab) & (column < 3 * slab)
        middle = nyquist & (column == 3 * slab)
        signed = jnp.where(odd, -1.0, 1.0)
        fold_ref[t] = jnp.where(direct, signed, jnp.where(mirror | middle, 1.0, 0.0)).astype(BF16)

    twist_copy.wait()
    filler = jnp.zeros((128 - 2 * row_count, block_len), F32)
    twist_ref[...] = jnp.transpose(jnp.concatenate([twist_in[...], filler], 0))
    w_copy.wait()
    wide = 256
    pieces = out_width // wide

    def fold_step(i, carry):
        base = pl.multiple_of((i // pieces) * group_len, group_len)
        cols = pl.ds(pl.multiple_of((i % pieces) * wide, wide), wide)
        for t in range(chips):
            high = min(group_len - slab * (t + 1), group_len - pair)
            taken = [w_ref[pl.ds(base + slab * t, slab), cols], w_ref[pl.ds(base + high, pair), cols]]
            if t == 0:
                taken.append(w_ref[pl.ds(base + group_len // 2, slab), cols])
            depth = slab * (4 if t == 0 else 3)
            folded[pl.ds(base + pair * t, pair), cols] = jnp.dot(
                fold_ref[t, :, :depth], jnp.concatenate(taken, 0), preferred_element_type=F32
            ).astype(BF16)
        return carry

    lax.fori_loop(0, col_count * pieces, fold_step, 0)

    def arrived(ref, semaphore):
        pltpu.make_async_remote_copy(
            src_ref=ref, dst_ref=ref, send_sem=l_sem.at[0], recv_sem=semaphore,
            device_id=(other, c), device_id_type=MESH,
        ).wait_recv()

    def block_of(d, i):
        return 2 * lax.rem(z - d + chips, chips) + i

    stay1.wait()
    low_copy.wait()
    arrived(recv1.at[other], a_recv.at[0])
    for d in range(1, chips):
        for i in range(2):
            arrived(recv1.at[block_of(d, i)], a_recv.at[2 * d + i])
    tile = 32
    lane = lax.broadcasted_iota(jnp.int32, (tile, slab), 1)
    sine = (lane > half) | ((lane == half) & (r > 0))

    def turn_step(i, carry):
        rows = pl.ds(pl.multiple_of(i * tile, tile), tile)
        below = pl.ds(pl.multiple_of(block_len + i * tile, tile), tile)
        blocks = [recv1[a, rows, :].astype(F32) for a in range(row_count)]
        middle = row_count // 2
        even = [blocks[a] + blocks[row_count - a] for a in range(1, middle)]
        odd = [blocks[a] - blocks[row_count - a] for a in range(1, middle)]
        ends = (blocks[0] + blocks[middle], blocks[0] - blocks[middle])
        twist = twist_ref[rows, :]
        for q in range(middle + 1):
            real = ends[q % 2]
            imag = None
            for a in range(1, middle):
                angle = 2 * math.pi * (a * q % row_count) / row_count
                cosine, sinus = round(math.cos(angle), 12), round(math.sin(angle), 12)
                if cosine:
                    real = real + even[a - 1] * cosine
                if sinus:
                    term = odd[a - 1] * -sinus
                    imag = term if imag is None else imag + term
            for k, sign in ((q, 1.0), (row_count - q, -1.0)):
                if k == row_count or (sign < 0 and k == q):
                    continue
                cosine, sinus = twist[:, k : k + 1], twist[:, row_count + k : row_count + k + 1]
                if imag is None:
                    turned_real, turned_imag = real * cosine, -(real * sinus)
                else:
                    turned_real = real * cosine + imag * (sinus * sign)
                    turned_imag = imag * (cosine * sign) - real * sinus
                cols = pl.ds(k * slab, slab)
                stacked[rows, cols] = jnp.where(sine, -turned_imag, turned_real).astype(BF16)
                stacked[below, cols] = jnp.where(sine, turned_real, turned_imag).astype(BF16)
        return carry

    lax.fori_loop(0, block_len // tile, turn_step, 0)

    def lanes_of(index):
        return pl.ds(pl.multiple_of(index * slab, slab), slab)

    sends = []

    def share(origin, source, block, target, out_slot, in_slot):
        copy = pltpu.make_async_remote_copy(
            src_ref=source, dst_ref=lhs.at[origin, :, :, lanes_of(block)],
            send_sem=g_send.at[out_slot], recv_sem=g_recv.at[in_slot],
            device_id=(r, target), device_id_type=MESH,
        )
        copy.start()
        sends.append(copy)
        return copy

    def held(origin, block):
        return lhs.at[origin, :, :, lanes_of(block)]

    count = row_count
    from_x, from_y, from_far = [], [], []

    def offer(n, source, block):
        from_x.append(share(c, source, block, x_next, n, n))
        from_y.append(share(c, source, block, y_next, count + n, count + n))

    second_copies = []
    stay2 = pltpu.make_async_copy(send2.at[r], held(c, r), l_sem.at[1])
    near_first = sorted(range(chips), key=lambda d: min(d, chips - d))
    for d in near_first:
        chip = lax.rem(z + d, chips)
        lows = jnp.dot(
            low_ref[pl.ds(pl.multiple_of(chip * 2 * part, 2 * part), 2 * part), :], stacked[...],
            preferred_element_type=F32,
        ).astype(BF16)
        for i in range(2):
            for q in range(row_count):
                send2[2 * chip + i, q] = lows[i * part : (i + 1) * part, q * slab : (q + 1) * slab]
        for target, slot in ([(2 * chip, 2 * d), (2 * chip + 1, 2 * d + 1)] if d else [(other, 0)]):
            copy = pltpu.make_async_remote_copy(
                src_ref=send2.at[target], dst_ref=held(c, r),
                send_sem=b_send.at[slot],
                recv_sem=b_recv.at[slot] if d == 0 else b_recv.at[2 * d + r % 2],
                device_id=(target, c), device_id_type=MESH,
            )
            copy.start()
            second_copies.append(copy)
        if d == 0:
            offer(0, send2.at[r], r)
            stay2.start()

    pairs = [lax.rem(z - d + chips, chips) for d in near_first]
    order = [(None, r), (0, other)]
    for d in near_first[1:]:
        order += [(2 * d + i, block_of(d, i)) for i in range(2)]

    def multiply(origin, m, first=False, last=False):
        base = pl.multiple_of(origin * group_len + pairs[m] * pair, pair)
        taken = pl.ds(pl.multiple_of(pairs[m] * pair, pair), pair)

        def step(i, carry):
            cols = pl.ds(pl.multiple_of(i * wide, wide), wide)
            left = lhs[origin, :, :, taken].reshape(block_len, pair)
            value = jnp.dot(left, folded[pl.ds(base, pair), cols], preferred_element_type=F32)
            if not first:
                value = acc[:, cols] + value
            if not last:
                acc[:, cols] = value
            else:
                out_ref[:, :, cols] = value.astype(BF16).reshape(row_count, part, wide)
            return carry

        lax.fori_loop(0, pieces, step, 0)

    def own_part(m):
        if m == 0:
            stay2.wait()
        multiply(c, m, first=m == 0)

    def x_part(m):
        from_x[2 * m + 1].wait_recv()
        multiply(x_next, m)

    def y_part(m):
        from_y[2 * m].wait_recv()
        multiply(y_next, m)

    def far_part(m):
        from_far[2 * m].wait_recv()
        from_far[2 * m + 1].wait_recv()
        multiply(diagonal, m, last=m == chips - 1)

    for n in range(1, count + 1):
        if n < count:
            slot, block = order[n]
            arrived(held(c, block), b_recv.at[slot])
            offer(n, held(c, block), block)
        _, block = order[n - 1]
        slot = 2 * count + n - 1
        if n % 2:
            from_x[n - 1].wait_recv()
            from_far.append(share(x_next, held(x_next, block), block, y_next, slot, slot))
        else:
            from_y[n - 1].wait_recv()
            from_far.append(share(y_next, held(y_next, block), block, x_next, slot, slot))
        m = n // 2
        if n % 2:
            own_part(m)
            if m:
                x_part(m - 1)
        elif 2 <= m < chips:
            y_part(m - 2)
            if m >= 3:
                far_part(m - 3)
    y_part(chips - 2)
    for m in range(max(chips - 3, 0), chips - 2):
        far_part(m)
    x_part(chips - 1)
    y_part(chips - 1)
    far_part(chips - 2)
    far_part(chips - 1)

    for copy in sum_copies + first_copies + second_copies + sends:
        copy.wait_send()


def on_device_fused(tokens, norm_gain, out_weight):
    row_count = lax.axis_size("row")
    col_count = lax.axis_size("col")
    block_len, group_len = tokens.shape
    out_width = out_weight.shape[1]
    slab = group_len // row_count
    part = block_len // row_count
    chan_table, low_table, twist_cos, twist_sin = host_tables(group_len, row_count, block_len)
    twist = np.concatenate([twist_cos, twist_sin], 0).astype(np.float32)
    vmem = pl.BlockSpec(memory_space=pltpu.VMEM)
    dma = pltpu.SemaphoreType.DMA
    mapped = pl.pallas_call(
        functools.partial(fused_kernel, (row_count, col_count)),
        out_shape=jax.ShapeDtypeStruct((row_count, part, out_width), BF16),
        in_specs=[vmem] * 2 + [pl.BlockSpec(memory_space=pl.ANY)] * 4,
        out_specs=vmem,
        scratch_shapes=[
            pltpu.VMEM(chan_table.shape, BF16),
            pltpu.VMEM(low_table.shape, BF16),
            pltpu.VMEM(twist.shape, F32),
            pltpu.VMEM((block_len, 128), F32),
            pltpu.VMEM(out_weight.shape, BF16),
            pltpu.VMEM((row_count // 2, 2 * slab, 4 * slab), BF16),
            pltpu.VMEM(out_weight.shape, BF16),
            pltpu.VMEM((row_count, block_len, slab), BF16),
            pltpu.VMEM((row_count, block_len, slab), BF16),
            pltpu.VMEM((col_count, 8, block_len), F32),
            pltpu.VMEM((2 * block_len, row_count * slab), BF16),
            pltpu.VMEM((row_count, row_count, part, slab), BF16),
            pltpu.VMEM((col_count, row_count, part, group_len), BF16),
            pltpu.VMEM((block_len, out_width), F32),
            dma, dma((col_count - 1,)), dma((col_count - 1,)),
            dma((row_count,)), dma((row_count,)), dma((row_count,)), dma((row_count,)),
            dma((3 * row_count,)), dma((3 * row_count,)), dma((5,)),
        ],
        compiler_params=pltpu.CompilerParams(
            collective_id=0, has_side_effects=True, vmem_limit_bytes=60 * 1024 * 1024
        ),
    )(
        tokens, norm_gain[None, :], jnp.asarray(chan_table, BF16), jnp.asarray(low_table, BF16),
        jnp.asarray(twist), out_weight,
    )
    return jnp.transpose(mapped, (1, 0, 2)).reshape(block_len, out_width)


def on_device(tokens, norm_gain, out_weight):
    row_count = lax.axis_size("row")
    col_count = lax.axis_size("col")
    block_len, local_width = tokens.shape
    full_width = local_width * col_count
    group_len = full_width // GROUPS
    share_len = block_len // col_count
    seq_len = block_len * row_count
    slab_len = full_width // row_count
    col_index = lax.axis_index("col")
    chan_idx = jnp.arange(group_len, dtype=jnp.int32)
    cosines, sines = phases(chan_idx, chan_idx, group_len)
    chan_table = jnp.concatenate([cosines, sines], axis=1) / math.sqrt(group_len)
    table_parts = split_table(chan_table)
    arranged = tokens.reshape(col_count, share_len, local_width)
    portion = lax.all_to_all(arranged, "col", split_axis=0, concat_axis=2, tiled=True)
    item_count = portion.shape[1]
    values = portion.astype(jnp.float32)
    inv_rms = lax.rsqrt(jnp.mean(values * values, axis=-1, keepdims=True) + EPSILON)
    normed = lax.optimization_barrier((values * inv_rms * norm_gain).astype(jnp.bfloat16))
    grouped = normed.reshape(item_count, GROUPS, group_len)
    result = jnp.einsum("pgm,mj->pgj", grouped, table_parts[0], preferred_element_type=jnp.float32)
    result = result + jnp.einsum(
        "pgm,mj->pgj", grouped, table_parts[1], preferred_element_type=jnp.float32
    )
    result = result + jnp.einsum(
        "pgm,mj->pgj", grouped, table_parts[2], preferred_element_type=jnp.float32
    )
    high_idx = jnp.arange(row_count, dtype=jnp.int32)
    high_cos, high_sin = phases(high_idx, high_idx, row_count)
    high_table = jnp.concatenate(
        [jnp.concatenate([high_cos, -high_sin], 1), jnp.concatenate([-high_sin, -high_cos], 1)], 0
    )
    parts = (
        lax.all_to_all(
            result[..., :group_len].reshape(1, item_count, full_width),
            "row",
            split_axis=2,
            concat_axis=0,
            tiled=True,
        ),
        lax.all_to_all(
            result[..., group_len:].reshape(1, item_count, full_width),
            "row",
            split_axis=2,
            concat_axis=0,
            tiled=True,
        ),
    )
    item_count = parts[0].shape[1]
    stacked = jnp.concatenate(parts, 0).reshape(2 * row_count, item_count * slab_len)
    result = jnp.dot(high_table, stacked, precision=PRECISE)
    real_part = result[:row_count].reshape(row_count, item_count, slab_len)
    imag_part = result[row_count:].reshape(row_count, item_count, slab_len)
    local_pos = col_index * share_len + jnp.arange(share_len, dtype=jnp.int32)
    twist_cos, twist_sin = phases(high_idx, local_pos, seq_len)
    twist_cos = twist_cos[:, :, None]
    twist_sin = twist_sin[:, :, None]
    turned_real = real_part * twist_cos + imag_part * twist_sin
    turned_imag = imag_part * twist_cos - real_part * twist_sin
    low_idx = jnp.arange(block_len, dtype=jnp.int32)
    low_cos, low_sin = phases(low_idx, low_idx, block_len)
    low_cos = low_cos / math.sqrt(seq_len)
    low_sin = low_sin / math.sqrt(seq_len)
    low_table = jnp.concatenate([low_cos, low_sin], 1)
    stacked = jnp.concatenate(
        (
            lax.all_to_all(turned_real, "col", split_axis=0, concat_axis=1, tiled=True),
            lax.all_to_all(turned_imag, "col", split_axis=0, concat_axis=1, tiled=True),
        ),
        1,
    )
    finished = (jnp.einsum("ks,asc->akc", low_table, stacked, precision=PRECISE),)[0]
    spectrum = finished.astype(jnp.bfloat16)
    returned = lax.all_to_all(spectrum, "row", split_axis=1, concat_axis=2, tiled=True)
    mapped = jnp.einsum(
        "akd,de->kae",
        lax.all_gather(returned, "col", axis=0, tiled=True),
        out_weight,
        preferred_element_type=jnp.float32,
    )
    return mapped.astype(jnp.bfloat16).reshape(block_len, local_width)


def solution(mesh):
    def body(tokens, norm_gain, out_weight):
        whole_groups = tokens.shape[1] * GROUPS == out_weight.shape[0]
        slab = tokens.shape[1] // mesh.shape["row"]
        program = on_device_folded if whole_groups else on_device
        if whole_groups and slab == 128 and mesh.shape["col"] == 4 and mesh.shape["row"] == 8:
            program = on_device_fused
        return program(tokens, norm_gain, out_weight)

    placed = (P("row", "col"), P(), P(None, "col"))
    return jax.shard_map(
        body, mesh=mesh, in_specs=placed, out_specs=P("row", "col"), check_vma=False
    )
```

profile of v0, /device:TPU:21, one launch (start us, length us, event | category | flops | bytes accessed | tf_op | source)
XLA Modules:
  0.0 85.2 jit_solution(4580366569070548923)
XLA Ops:
  0.0 82.5 %shard_map.64 = bf16[8,64,1024]{2,1,0:T(8,128)(2,1)} custom-call(bf16[512,1024]{1,0:T(8,128)(2,1)} %x_ref.1, f32[1,4096]{1,0:T(1,128)} %bitcast.6, bf16[1024,1024]{1,0:T(8,128)(2,1)} %constant.6.clone.table_hbm, bf16[512,1024]{1,0:T(8,128)(2,1)} %constant.7.clone.low_hbm, f32[16,512]{1,0:T(8,128)} %constant.8.clone.twist_hbm, bf16[4096,1024]{1,0:T(8,128)(2,1)} %w_hbm.1), custom_call_target="tpu_custom_call" | custom-call | tf_op jit(solution)/shard_map/pallas_call | solution.py:448
  82.5 2.8 %copy.9 = bf16[64,8,1024]{2,1,0:T(8,128)(2,1)} copy(bf16[64,8,1024]{2,0,1:T(8,128)(2,1)} %bitcast.5) | data formatting | bytes 2097152 | tf_op jit(solution)/shard_map/transpose | solution.py:479
where the time goes:
time: 85.4 us; the launch traced here: 85.2 us
  Pallas kernels  82.5 us (97%)
  local copies, waits for them, and re-layouts  2.77 us (3%)
    pallas_call x1, Pallas kernels, on_device_fused(): pl.pallas_call(functools.partial(fused_kernel, (row_count, col_count)), o...  82.5 us
    transpose x1, local copies, waits for them, and re-layouts, on_device_fused(): return jnp.transpose(mapped, (1, 0, 2)).reshape(block_len, out_width)  2.77 us

commit v1 on v0

v1 whole, which is shorter than its diff:
```python
import functools
import math

import numpy as np

import jax
import jax.numpy as jnp
from jax import lax
from jax.experimental import pallas as pl
from jax.experimental.pallas import tpu as pltpu
from jax.sharding import PartitionSpec as P

GROUPS = 4


EPSILON = 1e-06
PRECISE = lax.Precision.HIGHEST


def phases(left_idx, right_idx, period):
    product = left_idx[:, None] * right_idx[None, :] % period
    angles = product.astype(jnp.float32) * (2.0 * math.pi / period)
    return (jnp.cos(angles), jnp.sin(angles))


def split_table(table):
    table_high = table.astype(jnp.bfloat16)
    remainder = table - table_high.astype(jnp.float32)
    table_middle = remainder.astype(jnp.bfloat16)
    table_low = (remainder - table_middle.astype(jnp.float32)).astype(jnp.bfloat16)
    return (table_high, table_middle, table_low)


def host_tables(group_len, row_count, block_len):
    seq_len = block_len * row_count
    half = group_len // 2 // row_count
    slot = np.arange(group_len)
    freq = (slot // (2 * half)) * half + slot % half
    odd = slot // half % 2 == 1
    nyquist = odd & (freq == 0)
    sine = odd & ~nyquist
    freq = np.where(nyquist, group_len // 2, freq)
    chan = np.arange(group_len)
    angle = 2 * np.pi * (chan[:, None] * freq[None, :] % group_len) / group_len
    chan_table = np.where(sine[None, :], np.sin(angle), np.cos(angle)) / np.sqrt(group_len)
    low = np.arange(block_len)
    angle = 2 * np.pi * (low[:, None] * low[None, :] % block_len) / block_len
    low_table = np.concatenate([np.cos(angle), np.sin(angle)], 1) / np.sqrt(seq_len)
    high = np.arange(row_count)
    angle = 2 * np.pi * (high[:, None] * low[None, :] % seq_len) / seq_len
    return chan_table, low_table, np.cos(angle), np.sin(angle)


def slot_facts(slot, group_len, row_count):
    half = group_len // 2 // row_count
    freq = (slot // (2 * half)) * half + slot % half
    odd = slot // half % 2 == 1
    nyquist = odd & (freq == 0)
    return jnp.where(nyquist, group_len // 2, freq), odd & ~nyquist


def folding(group_len, row_count):
    freq, sine = slot_facts(jnp.arange(group_len, dtype=jnp.int32), group_len, row_count)
    chan = jnp.arange(group_len, dtype=jnp.int32)[None, :]
    direct = chan == freq[:, None]
    mirror = chan == ((group_len - freq) % group_len)[:, None]
    signed = jnp.where(sine[:, None], -1.0, 1.0)
    return jnp.where(direct, signed, jnp.where(mirror, 1.0, 0.0)).astype(jnp.bfloat16)


def on_device_folded(tokens, norm_gain, out_weight):
    row_count = lax.axis_size("row")
    col_count = lax.axis_size("col")
    block_len, group_len = tokens.shape
    full_width = group_len * col_count
    slab = group_len // row_count
    out_width = out_weight.shape[1]
    chan_table, low_table, twist_cos, twist_sin = host_tables(group_len, row_count, block_len)
    chan_table = jnp.asarray(chan_table, jnp.bfloat16)
    low_table = jnp.asarray(low_table, jnp.bfloat16)
    twist_cos = jnp.asarray(twist_cos, jnp.float32)[:, :, None]
    twist_sin = jnp.asarray(twist_sin, jnp.float32)[:, :, None]
    values = tokens.astype(jnp.float32)
    total = lax.psum(jnp.sum(values * values, axis=-1), "col")
    inv_rms = lax.rsqrt(total / full_width + EPSILON)[:, None]
    gain = lax.dynamic_slice_in_dim(norm_gain, lax.axis_index("col") * group_len, group_len)
    normed = (values * inv_rms * gain).astype(jnp.bfloat16)
    chans = jnp.dot(normed, chan_table, preferred_element_type=jnp.float32).astype(jnp.bfloat16)
    moved = lax.all_to_all(chans, "row", split_axis=1, concat_axis=0, tiled=True)
    blocks = moved.reshape(row_count, block_len, slab).astype(jnp.float32)
    _, sine = slot_facts(
        lax.axis_index("row") * slab + jnp.arange(slab, dtype=jnp.int32), group_len, row_count
    )
    tops, bottoms = [], []
    for q in range(row_count):
        real, imag = 0.0, 0.0
        for a in range(row_count):
            angle = 2 * math.pi * (a * q % row_count) / row_count
            real = real + blocks[a] * round(math.cos(angle), 12)
            imag = imag - blocks[a] * round(math.sin(angle), 12)
        turned_real = real * twist_cos[q] + imag * twist_sin[q]
        turned_imag = imag * twist_cos[q] - real * twist_sin[q]
        tops.append(jnp.where(sine, -turned_imag, turned_real).astype(jnp.bfloat16))
        bottoms.append(jnp.where(sine, turned_real, turned_imag).astype(jnp.bfloat16))
    stacked = jnp.concatenate([jnp.concatenate(tops, 1), jnp.concatenate(bottoms, 1)], 0)
    lows = jnp.dot(low_table, stacked, preferred_element_type=jnp.float32).astype(jnp.bfloat16)
    back = lax.all_to_all(
        lows.reshape(row_count, block_len // row_count, row_count * slab),
        "row", split_axis=0, concat_axis=0, tiled=True,
    )
    gathered = lax.all_gather(back, "col", axis=0, tiled=False)
    fold = folding(group_len, row_count)
    folded = jnp.einsum(
        "sm,gme->gse", fold, out_weight.reshape(col_count, group_len, out_width),
        preferred_element_type=jnp.float32,
    ).astype(jnp.bfloat16)
    mapped = jnp.einsum(
        "gspql,gsle->pqe",
        gathered.reshape(col_count, row_count, block_len // row_count, row_count, slab),
        folded.reshape(col_count, row_count, slab, out_width),
        preferred_element_type=jnp.float32,
    )
    return mapped.astype(jnp.bfloat16).reshape(block_len, out_width)


MESH = pl.DeviceIdType.MESH
F32 = jnp.float32
BF16 = jnp.bfloat16
WIDTHS = (16, 32, 32, 16, 16, 16)
NEAR_FIRST = (True, True, True, True, True, True)
FOLDS = (0, 6, 11, 16)
PLAN = (
    "A0", "A1", "F0", "I", "A2", "D0", "D1", "Gn0", "Gf0", "Gn1", "A3", "D2", "F1", "Xn0", "Xn1", "Gf1",
    "Xf0", "Gn2", "Xf1", "A4", "D3", "Gf2", "Xn2", "F2", "A5", "D4", "Gn3", "Mf0", "Gf3", "Mf1", "Xf2",
    "Mn0", "Xn3", "D5", "Xf3", "Gn4", "Mn1", "Gf4", "Mn3", "Gn5", "Mf3", "Xn4", "Xf4", "Mf2", "Gf5", "Xn5",
    "Mn2", "Mn4", "Xf5", "Mf4", "Mn5", "Mf5",
)


def fused_tables(group_len, row_count, block_len):
    seq_len = block_len * row_count
    freqs, sines = [], []
    offset = 0
    for width in WIDTHS:
        half = width // 2
        slot = np.arange(row_count * width)
        freqs.append(row_count // 2 * offset + slot // width * half + slot % half)
        sines.append(slot % width >= half)
        offset += width
    freq, odd = np.concatenate(freqs), np.concatenate(sines)
    nyquist = odd & (freq == 0)
    sine = odd & ~nyquist
    freq = np.where(nyquist, group_len // 2, freq)
    chan = np.arange(group_len)
    angle = 2 * np.pi * (freq[:, None] * chan[None, :] % group_len) / group_len
    chan_table = np.where(sine[:, None], np.sin(angle), np.cos(angle)) / np.sqrt(group_len)
    low = np.arange(block_len)
    angle = 2 * np.pi * (low[:, None] * low[None, :] % block_len) / block_len
    low_table = np.concatenate([np.cos(angle), np.sin(angle)], 0) / np.sqrt(seq_len)
    high = np.arange(row_count)
    angle = 2 * np.pi * (high[:, None] * low[None, :] % seq_len) / seq_len
    return chan_table, low_table, np.concatenate([np.cos(angle), np.sin(angle)], 0)


def fused_kernel(
    dims, x_hbm, gain_ref, table_hbm, low_hbm, twist_ref, w_hbm, out_ref,
    x_ref, scaled, table_ref, low_ref, w_ref, fold_ref, folded, send1, recv1, sums, invs, stacked, send2,
    held, lhs, acc,
    l_sem, stay_sem, send_sem, s_recv, i_recv, a_recv, b_recv, g_recv,
):
    row_count, col_count = dims
    block_len, group_len = x_ref.shape
    full_width = group_len * col_count
    out_width = out_ref.shape[2]
    part = block_len // row_count
    slab = group_len // row_count
    chunks = len(WIDTHS)
    offsets = [sum(WIDTHS[:i]) for i in range(chunks)]
    quads = row_count // 2
    r = lax.axis_index("row")
    c = lax.axis_index("col")
    core, inner, side = r % 2, r // 2 % 2, r // 4

    def peer_of(d):
        k = 1 - core if d % 2 else core
        t = 1 - inner if d // 2 % 2 else inner
        s = 1 - side if d // 4 else side
        return 4 * s + 2 * t + k

    x_next = 2 * (c // 2) + 1 - c % 2
    y_next = 2 * (1 - c // 2) + c % 2
    diagonal = 2 * (1 - c // 2) + 1 - c % 2
    col_peers = (x_next, y_next, diagonal)
    near, far = tuple(range(1, quads)), tuple(range(quads, row_count))

    def rows_of(start, size, unit):
        return pl.ds(pl.multiple_of(start, unit), size)

    x_copy = pltpu.make_async_copy(x_hbm, x_ref, l_sem.at[0])
    early = row_count * WIDTHS[0]
    table_copy = pltpu.make_async_copy(table_hbm.at[:early], table_ref.at[:early], l_sem.at[1])
    table_rest = pltpu.make_async_copy(table_hbm.at[early:], table_ref.at[early:], l_sem.at[4])
    low_copy = pltpu.make_async_copy(low_hbm, low_ref, l_sem.at[2])
    w_copy = pltpu.make_async_copy(w_hbm, w_ref, l_sem.at[3])
    x_copy.start()
    table_copy.start()

    barrier = pltpu.get_barrier_semaphore()
    for d in range(1, row_count):
        pl.semaphore_signal(barrier, inc=1, device_id=(peer_of(d), c), device_id_type=MESH)
    for peer in col_peers:
        pl.semaphore_signal(barrier, inc=1, device_id=(r, peer), device_id_type=MESH)

    lanes = (((1,), (1,)), ((), ()))
    x_copy.wait()
    for copy in (table_rest, low_copy, w_copy):
        copy.start()
    values = x_ref[...].astype(F32)
    gain = gain_ref[:, pl.ds(pl.multiple_of(c * group_len, group_len), group_len)]
    scaled[...] = (values * gain).astype(BF16)

    def remote(source, target_ref, phase, recv_sem, device):
        pltpu.make_async_remote_copy(
            src_ref=source, dst_ref=target_ref, send_sem=send_sem.at[phase], recv_sem=recv_sem,
            device_id=device, device_id_type=MESH,
        ).start()

    def sent(ref, phase):
        pltpu.make_async_remote_copy(
            src_ref=ref, dst_ref=ref, send_sem=send_sem.at[phase], recv_sem=l_sem.at[0],
            device_id=(peer_of(1), c), device_id_type=MESH,
        ).wait_send()

    def arrived(ref, semaphore):
        pltpu.make_async_remote_copy(
            src_ref=ref, dst_ref=ref, send_sem=l_sem.at[0], recv_sem=semaphore,
            device_id=(peer_of(1), c), device_id_type=MESH,
        ).wait_recv()

    first_stays, second_stays = {}, {}

    def features(i):
        width, offset = WIDTHS[i], offsets[i]
        rows = pl.ds(row_count * offset, row_count * width)
        send1[rows, :] = lax.dot_general(
            table_ref[rows, :], scaled[...], lanes, preferred_element_type=F32
        ).astype(BF16)

    def first_exchange(i):
        width, offset = WIDTHS[i], offsets[i]
        if i == 0:
            square_sums()
            table_copy.wait()
        if i == 1:
            table_rest.wait()
        features(i)
        if i == 0:
            pl.semaphore_wait(barrier, row_count + col_count - 2)
            for peer in col_peers:
                remote(sums.at[c], sums.at[c], 0, s_recv.at[0], (r, peer))
        target = recv1.at[r, pl.ds(offset, width), :]
        for d in far + near[::-1]:
            peer = peer_of(d)
            source = send1.at[rows_of(row_count * offset + peer * width, width, 16), :]
            remote(source, target, 2, a_recv.at[i], (peer, c))
        source = send1.at[rows_of(row_count * offset + r * width, width, 16), :]
        first_stays[i] = pltpu.make_async_copy(source, target, stay_sem.at[0, i])
        first_stays[i].start()

    def square_sums():
        squares = x_ref[...].astype(F32)
        squares = squares * squares
        top = squares.astype(BF16)
        rest = (squares - top.astype(F32)).astype(BF16)
        ones = jnp.ones((16, group_len), BF16)
        own = lax.dot_general(ones, top, lanes, preferred_element_type=F32)
        own = own + lax.dot_general(ones, rest, lanes, preferred_element_type=F32)
        sums[c] = own[:1]

    def inverses():
        arrived(sums.at[: col_count - 1], s_recv.at[0])
        total = sums[0]
        for k in range(1, col_count):
            total = total + sums[k]
        invs[r] = lax.rsqrt(total / full_width + EPSILON)
        for d in far + near[::-1]:
            remote(invs.at[r], invs.at[r], 1, i_recv.at[0], (peer_of(d), c))

    def butterfly(i):
        width, offset = WIDTHS[i], offsets[i]
        half = width // 2
        middle = row_count // 2

        def step(j, carry):
            spot = rows_of(j * 128, 128, 128)
            below = rows_of(block_len + j * 128, 128, 128)
            for base in range(0, width, 16):
                rows = pl.ds(offset + base, 16)
                blocks = [
                    recv1[a, rows, spot].astype(F32) * invs[a, :, spot] for a in range(row_count)
                ]
                even = [blocks[a] + blocks[row_count - a] for a in range(1, middle)]
                odd = [blocks[a] - blocks[row_count - a] for a in range(1, middle)]
                ends = (blocks[0] + blocks[middle], blocks[0] - blocks[middle])
                row = lax.broadcasted_iota(jnp.int32, (16, 128), 0) + base
                sine = row >= half
                if offset == 0:
                    sine = (row > half) | ((row == half) & (r > 0))
                plain = base + 16 <= half
                turned = base >= half and (offset > 0 or base > half)
                for q in range(middle + 1):
                    real = ends[q % 2]
                    imag = None
                    for a in range(1, middle):
                        angle = 2 * math.pi * (a * q % row_count) / row_count
                        cosine, sinus = round(math.cos(angle), 12), round(math.sin(angle), 12)
                        if cosine:
                            real = real + (even[a - 1] if cosine == 1 else even[a - 1] * cosine)
                        if sinus:
                            term = odd[a - 1] * -sinus
                            imag = term if imag is None else imag + term
                    for k, sign in ((q, 1.0), (row_count - q, -1.0)):
                        if k == row_count or (sign < 0 and k == q):
                            continue
                        if k == 0:
                            turned_real, turned_imag = real, jnp.zeros_like(real)
                        else:
                            cosine = twist_ref[k : k + 1, spot]
                            sinus = twist_ref[row_count + k : row_count + k + 1, spot]
                            if imag is None:
                                turned_real, turned_imag = real * cosine, -(real * sinus)
                            elif sign > 0:
                                turned_real = real * cosine + imag * sinus
                                turned_imag = imag * cosine - real * sinus
                            else:
                                turned_real = real * cosine - imag * sinus
                                turned_imag = -(imag * cosine + real * sinus)
                        if plain:
                            upper, lower = turned_real, turned_imag
                        elif turned:
                            upper, lower = -turned_imag, turned_real
                        else:
                            upper = jnp.where(sine, -turned_imag, turned_real)
                            lower = jnp.where(sine, turned_real, turned_imag)
                        place = pl.ds((k % 2 * quads + k // 2) * width + base, 16)
                        stacked[place, spot] = upper.astype(BF16)
                        stacked[place, below] = lower.astype(BF16)
            return carry

        lax.fori_loop(0, block_len // 128, step, 0)

    def second_exchange(i):
        width, offset = WIDTHS[i], offsets[i]
        lane = lax.broadcasted_iota(jnp.int32, (quads * width, 128), 1)
        first_half = lane < part
        target = held.at[c, :, rows_of(row_count * offset + r * width, width, 16), :]
        for nearby in (True, False) if NEAR_FIRST[i] else (False, True):
            where = side if nearby else 1 - side
            lows = jnp.dot(
                stacked[: row_count * width, :],
                low_ref[:, rows_of(where * (block_len // 2), block_len // 2, 256)],
                preferred_element_type=F32,
            )
            for t in range(2):
                left = lows[: quads * width, t * 128 : (t + 1) * 128]
                right = lows[quads * width :, t * 128 : (t + 1) * 128]
                pair = (
                    jnp.where(first_half, left, pltpu.roll(right, part, 1)),
                    jnp.where(first_half, pltpu.roll(left, part, 1), right),
                )
                for k in range(2):
                    value = pair[k].astype(BF16).reshape(quads, width, 128)
                    send2[4 * where + 2 * t + k, :, pl.ds(offset, width), :] = value
            for d in near[::-1] if nearby else far:
                peer = peer_of(d)
                source = send2.at[peer, :, pl.ds(offset, width), :]
                remote(source, target, 3, b_recv.at[i, 0 if nearby else 1], (peer, c))
        source = send2.at[r, :, pl.ds(offset, width), :]
        second_stays[i] = pltpu.make_async_copy(source, target, stay_sem.at[1, i])
        second_stays[i].start()

    def transform(i):
        width, offset = WIDTHS[i], offsets[i]
        first_stays[i].wait()
        if i == 0:
            low_copy.wait()
            arrived(invs.at[: row_count - 1], i_recv.at[0])
        arrived(recv1.at[: row_count - 1, pl.ds(offset, width), :], a_recv.at[i])
        butterfly(i)
        second_exchange(i)

    def place_of(i, h):
        width, offset = WIDTHS[i], offsets[i]
        where = side if h == "n" else 1 - side
        return rows_of(row_count * offset + where * quads * width, quads * width, 16)

    def piece(origin, i, h, u):
        return held.at[origin, pl.ds(2 * u, 2), place_of(i, h), :]

    def spread(i, h, u, origin, target, kind):
        slot = 2 * i + (h == "f")
        part_ref = piece(origin, i, h, u)
        remote(part_ref, part_ref, 4, g_recv.at[slot, kind], (r, target))

    def came(i, h, u, origin, kind):
        arrived(piece(origin, i, h, u), g_recv.at[2 * i + (h == "f"), kind])

    def gather(i, h):
        width, offset = WIDTHS[i], offsets[i]
        if h == "n":
            arrived(held.at[c, :, pl.ds(row_count * offset, len(near) * width), :], b_recv.at[i, 0])
            second_stays[i].wait()
        else:
            arrived(held.at[c, :, pl.ds(row_count * offset, len(far) * width), :], b_recv.at[i, 1])
        spread(i, h, 0, c, x_next, 0)
        spread(i, h, 1, c, y_next, 1)
        spread(i, h, 1, c, x_next, 2)
        spread(i, h, 0, c, y_next, 2)

    def forward(i, h):
        came(i, h, 0, x_next, 0)
        spread(i, h, 0, x_next, y_next, 2)
        came(i, h, 1, y_next, 1)
        spread(i, h, 1, y_next, x_next, 2)

    wide, broad = 256, 512
    pieces = out_width // wide

    def fold_spans(i):
        width, offset = WIDTHS[i], offsets[i]
        start, count = quads * offset, quads * width
        high = min(group_len - start - count, group_len - count - 16)
        return start, count, high, 2 * count + 16 + (16 if i == 0 else 0)

    def fold_matrix(i):
        width = WIDTHS[i]
        start, count, high, depth = fold_spans(i)
        shape = (2 * count, depth)
        slot = lax.broadcasted_iota(jnp.int32, shape, 0)
        column = lax.broadcasted_iota(jnp.int32, shape, 1)
        half = width // 2
        freq = start + slot // width * half + slot % half
        odd = slot % width >= half
        nyquist = odd & (freq == 0)
        direct = (column == freq - start) & ~nyquist & (column < count)
        mirror = (column - count + high == group_len - freq) & (freq > 0)
        mirror = mirror & (column >= count) & (column < 2 * count + 16)
        middle = nyquist & (column == 2 * count + 16)
        signed = jnp.where(odd, -1.0, 1.0)
        matrix = jnp.where(direct, signed, jnp.where(mirror | middle, 1.0, 0.0)).astype(BF16)
        fold_ref[row_count * offsets[i] : row_count * (offsets[i] + width), :depth] = matrix

    def fold(m):
        if m == 0:
            for i in range(chunks):
                fold_matrix(i)
            w_copy.wait()

        def step(n, carry):
            group = n // pieces
            origin = group * group_len
            cols = rows_of(n % pieces * wide, wide, wide)
            for i in range(chunks):
                start, count, high, depth = fold_spans(i)
                base = row_count * offsets[i]
                taken = [w_ref[rows_of(origin + start, count, 16), cols]]
                taken.append(w_ref[rows_of(origin + high, count + 16, 16), cols])
                if i == 0:
                    taken.append(w_ref[rows_of(origin + group_len // 2, 16, 16), cols])
                value = jnp.dot(
                    fold_ref[base : base + 2 * count, :depth], jnp.concatenate(taken, 0),
                    preferred_element_type=F32,
                ).astype(BF16)
                for s in range(2):
                    start = base * col_count + s * col_count * count + group * count
                    folded[rows_of(start, count, 16), cols] = value[s * count : (s + 1) * count]
            return carry

        lax.fori_loop(FOLDS[m], FOLDS[m + 1], step, 0)

    done = []

    def multiply(i, h):
        width, offset = WIDTHS[i], offsets[i]
        count = quads * width
        depth = col_count * count
        arrived(held.at[:2, :, place_of(i, h), :], g_recv.at[2 * i + (h == "f"), 2])
        for g in range(col_count):
            for q in range(quads):
                lhs[q * 128 : (q + 1) * 128, g * count : (g + 1) * count] = jnp.transpose(
                    held[g, q, place_of(i, h), :]
                )
        where = side if h == "n" else 1 - side
        rows = rows_of(row_count * offset * col_count + where * depth, depth, 16)
        first, last = not done, len(done) == 2 * chunks - 1
        done.append((i, h))

        def step(n, carry):
            cols = rows_of(n * broad, broad, broad)
            value = jnp.dot(lhs[:, :depth], folded[rows, cols], preferred_element_type=F32)
            if not first:
                value = acc[:, cols] + value
            if not last:
                acc[:, cols] = value
            else:
                out_ref[:, :, cols] = value.astype(BF16).reshape(row_count, part, broad)
            return carry

        lax.fori_loop(0, out_width // broad, step, 0)

    for token in PLAN:
        i = int(token[-1]) if token[-1].isdigit() else 0
        with jax.named_scope(token):
            match token[0]:
                case "A":
                    first_exchange(i)
                case "I":
                    inverses()
                case "F":
                    fold(i)
                case "D":
                    transform(i)
                case "G":
                    gather(i, token[1])
                case "X":
                    forward(i, token[1])
                case "M":
                    multiply(i, token[1])

    sent(sums.at[: col_count - 1], 0)
    sent(invs.at[: row_count - 1], 1)
    sent(send1.at[: group_len - slab], 2)
    sent(send2.at[: row_count - 1], 3)
    sent(held.at[: col_count - 1], 4)


def on_device_fused(tokens, norm_gain, out_weight):
    row_count = lax.axis_size("row")
    col_count = lax.axis_size("col")
    block_len, group_len = tokens.shape
    out_width = out_weight.shape[1]
    slab = group_len // row_count
    part = block_len // row_count
    chunks = len(WIDTHS)
    widest = max(WIDTHS)
    chan_table, low_table, twist = fused_tables(group_len, row_count, block_len)
    vmem = pl.BlockSpec(memory_space=pltpu.VMEM)
    hbm = pl.BlockSpec(memory_space=pl.ANY)
    dma = pltpu.SemaphoreType.DMA
    mapped = pl.pallas_call(
        functools.partial(fused_kernel, (row_count, col_count)),
        out_shape=pltpu.VMEM((row_count, part, out_width), BF16),
        in_specs=[hbm, vmem, hbm, hbm, vmem, hbm],
        out_specs=vmem,
        scratch_shapes=[
            pltpu.VMEM((block_len, group_len), BF16),
            pltpu.VMEM((block_len, group_len), BF16),
            pltpu.VMEM(chan_table.shape, BF16),
            pltpu.VMEM(low_table.shape, BF16),
            pltpu.VMEM(out_weight.shape, BF16),
            pltpu.VMEM((group_len, row_count * widest + 32), BF16),
            pltpu.VMEM(out_weight.shape, BF16),
            pltpu.VMEM((group_len, block_len), BF16),
            pltpu.VMEM((row_count, slab, block_len), BF16),
            pltpu.VMEM((col_count, 1, block_len), F32),
            pltpu.VMEM((row_count, 1, block_len), F32),
            pltpu.VMEM((row_count * widest, 2 * block_len), BF16),
            pltpu.VMEM((row_count, row_count // 2, slab, 128), BF16),
            pltpu.VMEM((col_count, row_count // 2, group_len, 128), BF16),
            pltpu.VMEM((block_len, col_count * row_count // 2 * widest), BF16),
            pltpu.VMEM((block_len, out_width), F32),
            dma((5,)), dma((2, chunks)), dma((5,)), dma((1,)), dma((1,)),
            dma((chunks,)), dma((chunks, 2)), dma((2 * chunks, 3)),
        ],
        compiler_params=pltpu.CompilerParams(
            collective_id=0, has_side_effects=True, vmem_limit_bytes=60 * 1024 * 1024
        ),
    )(
        tokens, norm_gain[None, :], jnp.asarray(chan_table, BF16), jnp.asarray(low_table, BF16),
        jnp.asarray(twist, F32), out_weight,
    )
    return jnp.transpose(mapped, (1, 0, 2)).reshape(block_len, out_width)


def on_device(tokens, norm_gain, out_weight):
    row_count = lax.axis_size("row")
    col_count = lax.axis_size("col")
    block_len, local_width = tokens.shape
    full_width = local_width * col_count
    group_len = full_width // GROUPS
    share_len = block_len // col_count
    seq_len = block_len * row_count
    slab_len = full_width // row_count
    col_index = lax.axis_index("col")
    chan_idx = jnp.arange(group_len, dtype=jnp.int32)
    cosines, sines = phases(chan_idx, chan_idx, group_len)
    chan_table = jnp.concatenate([cosines, sines], axis=1) / math.sqrt(group_len)
    table_parts = split_table(chan_table)
    arranged = tokens.reshape(col_count, share_len, local_width)
    portion = lax.all_to_all(arranged, "col", split_axis=0, concat_axis=2, tiled=True)
    item_count = portion.shape[1]
    values = portion.astype(jnp.float32)
    inv_rms = lax.rsqrt(jnp.mean(values * values, axis=-1, keepdims=True) + EPSILON)
    normed = lax.optimization_barrier((values * inv_rms * norm_gain).astype(jnp.bfloat16))
    grouped = normed.reshape(item_count, GROUPS, group_len)
    result = jnp.einsum("pgm,mj->pgj", grouped, table_parts[0], preferred_element_type=jnp.float32)
    result = result + jnp.einsum(
        "pgm,mj->pgj", grouped, table_parts[1], preferred_element_type=jnp.float32
    )
    result = result + jnp.einsum(
        "pgm,mj->pgj", grouped, table_parts[2], preferred_element_type=jnp.float32
    )
    high_idx = jnp.arange(row_count, dtype=jnp.int32)
    high_cos, high_sin = phases(high_idx, high_idx, row_count)
    high_table = jnp.concatenate(
        [jnp.concatenate([high_cos, -high_sin], 1), jnp.concatenate([-high_sin, -high_cos], 1)], 0
    )
    parts = (
        lax.all_to_all(
            result[..., :group_len].reshape(1, item_count, full_width),
            "row",
            split_axis=2,
            concat_axis=0,
            tiled=True,
        ),
        lax.all_to_all(
            result[..., group_len:].reshape(1, item_count, full_width),
            "row",
            split_axis=2,
            concat_axis=0,
            tiled=True,
        ),
    )
    item_count = parts[0].shape[1]
    stacked = jnp.concatenate(parts, 0).reshape(2 * row_count, item_count * slab_len)
    result = jnp.dot(high_table, stacked, precision=PRECISE)
    real_part = result[:row_count].reshape(row_count, item_count, slab_len)
    imag_part = result[row_count:].reshape(row_count, item_count, slab_len)
    local_pos = col_index * share_len + jnp.arange(share_len, dtype=jnp.int32)
    twist_cos, twist_sin = phases(high_idx, local_pos, seq_len)
    twist_cos = twist_cos[:, :, None]
    twist_sin = twist_sin[:, :, None]
    turned_real = real_part * twist_cos + imag_part * twist_sin
    turned_imag = imag_part * twist_cos - real_part * twist_sin
    low_idx = jnp.arange(block_len, dtype=jnp.int32)
    low_cos, low_sin = phases(low_idx, low_idx, block_len)
    low_cos = low_cos / math.sqrt(seq_len)
    low_sin = low_sin / math.sqrt(seq_len)
    low_table = jnp.concatenate([low_cos, low_sin], 1)
    stacked = jnp.concatenate(
        (
            lax.all_to_all(turned_real, "col", split_axis=0, concat_axis=1, tiled=True),
            lax.all_to_all(turned_imag, "col", split_axis=0, concat_axis=1, tiled=True),
        ),
        1,
    )
    finished = (jnp.einsum("ks,asc->akc", low_table, stacked, precision=PRECISE),)[0]
    spectrum = finished.astype(jnp.bfloat16)
    returned = lax.all_to_all(spectrum, "row", split_axis=1, concat_axis=2, tiled=True)
    mapped = jnp.einsum(
        "akd,de->kae",
        lax.all_gather(returned, "col", axis=0, tiled=True),
        out_weight,
        preferred_element_type=jnp.float32,
    )
    return mapped.astype(jnp.bfloat16).reshape(block_len, local_width)


def solution(mesh):
    def body(tokens, norm_gain, out_weight):
        whole_groups = tokens.shape[1] * GROUPS == out_weight.shape[0]
        slab = tokens.shape[1] // mesh.shape["row"]
        program = on_device_folded if whole_groups else on_device
        if whole_groups and slab == 128 and mesh.shape["col"] == 4 and mesh.shape["row"] == 8:
            program = on_device_fused
        return program(tokens, norm_gain, out_weight)

    placed = (P("row", "col"), P(), P(None, "col"))
    return jax.shard_map(
        body, mesh=mesh, in_specs=placed, out_specs=P("row", "col"), check_vma=False
    )
```

time: 85.4 us -> 66.6 us (0.78)
  the two profiles are of different devices: /device:TPU:21 before, /device:TPU:0 now
where the time goes in v1:
time: 66.6 us; the launch traced here: 66.3 us
  Pallas kernels  64.8 us (97%)
  local copies, waits for them, and re-layouts  1.55 us (2%)
    pallas_call x1, Pallas kernels, on_device_fused(): pl.pallas_call(functools.partial(fused_kernel, (row_count, col_count)), o...  64.8 us
    transpose x1, local copies, waits for them, and re-layouts, on_device_fused(): return jnp.transpose(mapped, (1, 0, 2)).reshape(block_len, out_width)  1.55 us

profile of v1, /device:TPU:0, one launch (start us, length us, event | category | flops | bytes accessed | tf_op | source)
XLA Modules:
  0.0 66.3 jit_solution(4070130540089782523)
XLA Ops:
  0.0 64.8 %shard_map.64 = bf16[8,64,1024]{2,1,0:T(8,128)(2,1)S(1)} custom-call(bf16[512,1024]{1,0:T(8,128)(2,1)} %x_hbm.1, f32[1,4096]{1,0:T(1,128)} %bitcast.6, bf16[1024,1024]{1,0:T(8,128)(2,1)} %constant.6.clone.table_hbm, bf16[1024,512]{1,0:T(8,128)(2,1)} %constant.7.clone.low_hbm, f32[16,512]{1,0:T(8,128)} %constant.8.clone.twist_ref, bf16[4096,1024]{1,0:T(8,128)(2,1)} %w_hbm.1), custom_call_target="tpu_custom_call" | custom-call | tf_op jit(solution)/shard_map/pallas_call | solution.py:550
  64.8 1.5 %copy.9 = bf16[64,8,1024]{2,1,0:T(8,128)(2,1)} copy(bf16[64,8,1024]{2,0,1:T(8,128)(2,1)S(1)} %bitcast.5) | data formatting | bytes 2097152 | tf_op jit(solution)/shard_map/transpose | solution.py:582

commit v2 on v1

--- a/solution.py
+++ b/solution.py
@@ -127,13 +127,13 @@
 F32 = jnp.float32
 BF16 = jnp.bfloat16
 WIDTHS = (16, 32, 32, 16, 16, 16)
-NEAR_FIRST = (True, True, True, True, True, True)
+NEAR_FIRST = (True, True, True, False, True, True)
 FOLDS = (0, 6, 11, 16)
 PLAN = (
-    "A0", "A1", "F0", "I", "A2", "D0", "D1", "Gn0", "Gf0", "Gn1", "A3", "D2", "F1", "Xn0", "Xn1", "Gf1",
-    "Xf0", "Gn2", "Xf1", "A4", "D3", "Gf2", "Xn2", "F2", "A5", "D4", "Gn3", "Mf0", "Gf3", "Mf1", "Xf2",
-    "Mn0", "Xn3", "D5", "Xf3", "Gn4", "Mn1", "Gf4", "Mn3", "Gn5", "Mf3", "Xn4", "Xf4", "Mf2", "Gf5", "Xn5",
-    "Mn2", "Mn4", "Xf5", "Mf4", "Mn5", "Mf5",
+    "A0", "A1", "I", "A2", "D0", "D1", "F0", "Gn0", "A3", "Gf0", "Gn1", "Xf0", "D2", "Xn1", "Gf1", "Gn2",
+    "F1", "A4", "Xn0", "D3", "Xf1", "Xn2", "F2", "Gf2", "A5", "Gn3", "D4", "Xf2", "Mn1", "Gf3", "Mn2", "D5",
+    "Xn3", "Gn4", "Xf3", "Gn5", "Mn0", "Gf4", "Xn4", "Mf0", "Mf1", "Gf5", "Mn3", "Xf4", "Xn5", "Mf2", "Mn4",
+    "Xf5", "Mf3", "Mf4", "Mn5", "Mf5",
 )
 
 
@@ -163,8 +163,8 @@
 
 
 def fused_kernel(
-    dims, x_hbm, gain_ref, table_hbm, low_hbm, twist_ref, w_hbm, out_ref,
-    x_ref, scaled, table_ref, low_ref, w_ref, fold_ref, folded, send1, recv1, sums, invs, stacked, send2,
+    dims, x_hbm, gain_hbm, table_hbm, low_hbm, twist_hbm, w_hbm, out_ref,
+    x_ref, gain_ref, twist_ref, scaled, table_ref, low_ref, w_ref, fold_ref, folded, send1, recv1, sums, invs, stacked, send2,
     held, lhs, acc,
     l_sem, stay_sem, send_sem, s_recv, i_recv, a_recv, b_recv, g_recv,
 ):
@@ -202,8 +202,12 @@
     table_rest = pltpu.make_async_copy(table_hbm.at[early:], table_ref.at[early:], l_sem.at[4])
     low_copy = pltpu.make_async_copy(low_hbm, low_ref, l_sem.at[2])
     w_copy = pltpu.make_async_copy(w_hbm, w_ref, l_sem.at[3])
-    x_copy.start()
-    table_copy.start()
+    gain_copy = pltpu.make_async_copy(
+        gain_hbm.at[:, pl.ds(pl.multiple_of(c * group_len, group_len), group_len)], gain_ref, l_sem.at[5]
+    )
+    twist_copy = pltpu.make_async_copy(twist_hbm, twist_ref, l_sem.at[6])
+    for copy in (x_copy, gain_copy, table_copy):
+        copy.start()
 
     barrier = pltpu.get_barrier_semaphore()
     for d in range(1, row_count):
@@ -213,11 +217,10 @@
 
     lanes = (((1,), (1,)), ((), ()))
     x_copy.wait()
-    for copy in (table_rest, low_copy, w_copy):
+    for copy in (table_rest, low_copy, twist_copy, w_copy):
         copy.start()
-    values = x_ref[...].astype(F32)
-    gain = gain_ref[:, pl.ds(pl.multiple_of(c * group_len, group_len), group_len)]
-    scaled[...] = (values * gain).astype(BF16)
+    gain_copy.wait()
+    scaled[...] = (x_ref[...].astype(F32) * gain_ref[...]).astype(BF16)
 
     def remote(source, target_ref, phase, recv_sem, device):
         pltpu.make_async_remote_copy(
@@ -384,6 +387,7 @@
         first_stays[i].wait()
         if i == 0:
             low_copy.wait()
+            twist_copy.wait()
             arrived(invs.at[: row_count - 1], i_recv.at[0])
         arrived(recv1.at[: row_count - 1, pl.ds(offset, width), :], a_recv.at[i])
         butterfly(i)
@@ -550,10 +554,12 @@
     mapped = pl.pallas_call(
         functools.partial(fused_kernel, (row_count, col_count)),
         out_shape=pltpu.VMEM((row_count, part, out_width), BF16),
-        in_specs=[hbm, vmem, hbm, hbm, vmem, hbm],
+        in_specs=[hbm] * 6,
         out_specs=vmem,
         scratch_shapes=[
             pltpu.VMEM((block_len, group_len), BF16),
+            pltpu.VMEM((1, group_len), F32),
+            pltpu.VMEM(twist.shape, F32),
             pltpu.VMEM((block_len, group_len), BF16),
             pltpu.VMEM(chan_table.shape, BF16),
             pltpu.VMEM(low_table.shape, BF16),
@@ -569,7 +575,7 @@
             pltpu.VMEM((col_count, row_count // 2, group_len, 128), BF16),
             pltpu.VMEM((block_len, col_count * row_count // 2 * widest), BF16),
             pltpu.VMEM((block_len, out_width), F32),
-            dma((5,)), dma((2, chunks)), dma((5,)), dma((1,)), dma((1,)),
+            dma((7,)), dma((2, chunks)), dma((5,)), dma((1,)), dma((1,)),
             dma((chunks,)), dma((chunks, 2)), dma((2 * chunks, 3)),
         ],
         compiler_params=pltpu.CompilerParams(

time: 66.6 us -> 65.7 us (0.986)
  Pallas kernels: 64.8 us -> 64 us
    pallas_call x1, Pallas kernels: 64.8 us -> 64 us  [on_device_fused(): pl.pallas_call(functools.partial(fused_kernel, (row_count, col_count)), o...]
where the time goes in v2:
time: 65.7 us; the launch traced here: 65.5 us
  Pallas kernels  64 us (97%)
  local copies, waits for them, and re-layouts  1.55 us (2%)
    pallas_call x1, Pallas kernels, on_device_fused(): pl.pallas_call(functools.partial(fused_kernel, (row_count, col_count)), o...  64 us
    transpose x1, local copies, waits for them, and re-layouts, on_device_fused(): return jnp.transpose(mapped, (1, 0, 2)).reshape(block_len, out_width)  1.55 us

profile of v2, /device:TPU:0, one launch (start us, length us, event | category | flops | bytes accessed | tf_op | source)
XLA Modules:
  0.0 65.5 jit_solution(14317983361983674829)
XLA Ops:
  0.0 64.0 %shard_map.64 = bf16[8,64,1024]{2,1,0:T(8,128)(2,1)S(1)} custom-call(bf16[512,1024]{1,0:T(8,128)(2,1)} %x_hbm.1, f32[1,4096]{1,0:T(1,128)} %bitcast.6, bf16[1024,1024]{1,0:T(8,128)(2,1)} %constant.6.clone.table_hbm, bf16[1024,512]{1,0:T(8,128)(2,1)} %constant.7.clone.low_hbm, f32[16,512]{1,0:T(8,128)} %constant.8.clone.twist_hbm, bf16[4096,1024]{1,0:T(8,128)(2,1)} %w_hbm.1), custom_call_target="tpu_custom_call" | custom-call | tf_op jit(solution)/shard_map/pallas_call | solution.py:554
  64.0 1.5 %copy.9 = bf16[64,8,1024]{2,1,0:T(8,128)(2,1)} copy(bf16[64,8,1024]{2,0,1:T(8,128)(2,1)S(1)} %bitcast.5) | data formatting | bytes 2097152 | tf_op jit(solution)/shard_map/transpose | solution.py:588

commit v3 on v2

--- a/solution.py
+++ b/solution.py
@@ -252,15 +252,12 @@
     def first_exchange(i):
         width, offset = WIDTHS[i], offsets[i]
         if i == 0:
-            square_sums()
             table_copy.wait()
         if i == 1:
             table_rest.wait()
         features(i)
         if i == 0:
             pl.semaphore_wait(barrier, row_count + col_count - 2)
-            for peer in col_peers:
-                remote(sums.at[c], sums.at[c], 0, s_recv.at[0], (r, peer))
         target = recv1.at[r, pl.ds(offset, width), :]
         for d in far + near[::-1]:
             peer = peer_of(d)
@@ -269,6 +266,10 @@
         source = send1.at[rows_of(row_count * offset + r * width, width, 16), :]
         first_stays[i] = pltpu.make_async_copy(source, target, stay_sem.at[0, i])
         first_stays[i].start()
+        if i == 0:
+            square_sums()
+            for peer in col_peers:
+                remote(sums.at[c], sums.at[c], 0, s_recv.at[0], (r, peer))
 
     def square_sums():
         squares = x_ref[...].astype(F32)

time: 65.7 us -> 65.9 us (level)
  no operation moved by 1% of the time
where the time goes in v3:
time: 65.9 us; the launch traced here: 65.8 us
  Pallas kernels  64.2 us (97%)
  local copies, waits for them, and re-layouts  1.55 us (2%)
    pallas_call x1, Pallas kernels, on_device_fused(): pl.pallas_call(functools.partial(fused_kernel, (row_count, col_count)), o...  64.2 us
    transpose x1, local copies, waits for them, and re-layouts, on_device_fused(): return jnp.transpose(mapped, (1, 0, 2)).reshape(block_len, out_width)  1.55 us

profile of v3, /device:TPU:0, one launch (start us, length us, event | category | flops | bytes accessed | tf_op | source)
XLA Modules:
  0.0 65.8 jit_solution(8293425376895583127)
XLA Ops:
  0.0 64.2 %shard_map.64 = bf16[8,64,1024]{2,1,0:T(8,128)(2,1)S(1)} custom-call(bf16[512,1024]{1,0:T(8,128)(2,1)} %x_hbm.1, f32[1,4096]{1,0:T(1,128)} %bitcast.6, bf16[1024,1024]{1,0:T(8,128)(2,1)} %constant.6.clone.table_hbm, bf16[1024,512]{1,0:T(8,128)(2,1)} %constant.7.clone.low_hbm, f32[16,512]{1,0:T(8,128)} %constant.8.clone.twist_hbm, bf16[4096,1024]{1,0:T(8,128)(2,1)} %w_hbm.1), custom_call_target="tpu_custom_call" | custom-call | tf_op jit(solution)/shard_map/pallas_call | solution.py:555
  64.3 1.5 %copy.9 = bf16[64,8,1024]{2,1,0:T(8,128)(2,1)} copy(bf16[64,8,1024]{2,0,1:T(8,128)(2,1)S(1)} %bitcast.5) | data formatting | bytes 2097152 | tf_op jit(solution)/shard_map/transpose | solution.py:589
